TPU v7x, 32 devices: a whole 2x2x4 slice. The times are simulated.
32 devices in a mesh: ep: 4 (over y, x), tp: 8 (over z, core).
Axes of the slice: x: 2, y: 2, z: 4, core: 2. Of those that a mesh axis runs over, the one named last changes fastest.
Arguments:
- tokens: bfloat16 [64, 4096], P('ep'), may hold values from -6 to 6
- query_weight: bfloat16 [4096, 4096], P('ep', 'tp'), may hold values from -0.09375 to 0.09375
- key_weight: bfloat16 [4096, 2048], P('ep', 'tp'), may hold values from -0.15625 to 0.15625
- value_weight: bfloat16 [4096, 2048], P('ep', 'tp'), may hold values from -0.09375 to 0.09375
- out_weight: bfloat16 [4096, 4096], P('tp', 'ep'), may hold values from -0.09375 to 0.09375
- head_lambda: float32 [32], P('tp'), may hold values from 0.3 to 0.8
- head_gain: float32 [128], replicated, may hold values from 0.1 to 1.9
- key_cache: bfloat16 [64, 1024, 16, 128], P('ep', None, 'tp'), may hold values from -1000 to 1000
- value_cache: bfloat16 [64, 1024, 16, 128], P('ep', None, 'tp'), may hold values from -6 to 6
- lengths: int32 [64], P('ep'), may hold values from 128 to 1024, as said below
- first_gain: float32 [4096], replicated, may hold values from 0.3 to 3
- second_gain: float32 [4096], P('tp'), may hold values from 0.1 to 1.9
- expert_ids: int32 [64, 2], P('ep'), may hold values from 0 to 15, all different within a row; in each aligned block of 16 rows (0 to 15, 16 to 31, ...) at most 4 rows name the same one
- route_weights: float32 [64, 2], P('ep'), may hold values from 0.1 to 1
- expert_gate: bfloat16 [16, 4096, 2048], P('ep', 'tp'), may hold values from -0.09375 to 0.09375
- expert_up: bfloat16 [16, 4096, 2048], P('ep', 'tp'), may hold values from -0.09375 to 0.09375
- expert_down: bfloat16 [16, 2048, 4096], P('ep', None, 'tp'), may hold values from -0.125 to 0.125
- dense_gate: bfloat16 [4096, 2048], P('tp', 'ep'), may hold values from -0.09375 to 0.09375
- dense_up: bfloat16 [4096, 2048], P('tp', 'ep'), may hold values from -0.09375 to 0.09375
- dense_down: bfloat16 [2048, 4096], P('ep', 'tp'), may hold values from -0.25 to 0.25
- dense_mix: bfloat16 [4096], replicated, may hold values from -0.09375 to 0.09375
Outputs:
- layer_out: bfloat16 [64, 4096], P('ep', 'tp')
Inputs may be any that keep to these rules, and one draw needn't show every extreme that they name: `lengths`: positions below a sequence's length hold its cache; the new token stands at that position. Some sequence has length 1024 in every draw. `expert_ids`: each row names 2 different experts. Among the rows of one device's 16 sequences (aligned blocks) no expert is named more than 4 times, and in every draw some expert is named exactly 4 times in some block.
All inputs are finite; a program needn't handle non-finite values.
Results may differ from a plain program's by a relative error of at most 0.04.
Values may be sent and summed in bfloat16 or wider, within the bound.
A program may use at most 128 MiB of HBM per device.

v0:
```python
import jax
import jax.numpy as jnp
from jax import lax
from jax.sharding import PartitionSpec as P

SUB = 64
VD = 128
EXPERTS = 16
TOPK = 2
CACHE = 1024
CAP = 4


theta_base = 500000.0
score_scale = 0.125
head_scale = 0.8
residual_scale = 2.0**0.5
layer_epsilon = 1e-05
head_epsilon = 1e-06


def rotate(vector, cosine, sine_table):
    middle = vector.shape[-1] // 2
    lower = vector[..., :middle]
    upper = vector[..., middle:]
    return jnp.concatenate(
        [lower * cosine - upper * sine_table, upper * cosine + lower * sine_table], axis=-1
    )


def widened(array):
    return lax.optimization_barrier(array.astype(jnp.bfloat16)).astype(jnp.float32)


def attend(query_sum, key_sum, value_sum, head_lambda, head_gain, key_cache, value_cache, lengths):
    seq_count = key_cache.shape[0]
    kv_local = key_cache.shape[2]
    group_size = query_sum.shape[1] // (kv_local * 2 * SUB)
    frequency = theta_base ** (-(jnp.arange(SUB // 2, dtype=jnp.float32) * (2.0 / SUB)))
    angles = lengths.astype(jnp.float32)[:, None] * frequency[None, :]
    cosine = jnp.cos(angles)
    sine_table = jnp.sin(angles)
    query_half = widened(query_sum).reshape(seq_count, kv_local, group_size, 2, SUB)
    query_rot = rotate(
        query_half, cosine[:, None, None, None, :], sine_table[:, None, None, None, :]
    )
    query_rot = query_rot.astype(jnp.bfloat16)
    key_half = widened(key_sum).reshape(seq_count, kv_local, 2, SUB)
    key_rot = rotate(key_half, cosine[:, None, None, :], sine_table[:, None, None, :]).astype(
        jnp.bfloat16
    )
    value_new = widened(value_sum).reshape(seq_count, kv_local, 1, VD)
    cached_keys = key_cache.reshape(seq_count, CACHE, kv_local, 2, SUB)
    scores = jnp.einsum(
        "skgcd,sjkcd->skgcj", query_rot, cached_keys, preferred_element_type=jnp.float32
    )
    scores = scores * score_scale
    valid = jnp.arange(CACHE, dtype=jnp.int32)[None, :] < lengths[:, None]
    scores = jnp.where(valid[:, None, None, None, :], scores, -jnp.inf)
    fresh_score = jnp.einsum(
        "skgcd,skcd->skgc", query_rot, key_rot, preferred_element_type=jnp.float32
    )
    fresh_score = fresh_score * score_scale
    highest = jnp.maximum(jnp.max(scores, axis=-1), fresh_score)
    cached_exp = jnp.exp(scores - highest[..., None])
    fresh_exp = jnp.exp(fresh_score - highest)
    denominator = jnp.sum(cached_exp, axis=-1) + fresh_exp
    cached_prob = cached_exp / denominator[..., None]
    fresh_prob = fresh_exp / denominator
    lambdas = head_lambda.reshape(kv_local, group_size)
    mixed_map = (
        cached_prob[:, :, :, 0] - lambdas[None, :, :, None] * cached_prob[:, :, :, 1]
    ).astype(jnp.bfloat16)
    mixed_new = widened(fresh_prob[..., 0] - lambdas[None] * fresh_prob[..., 1])
    head_out = jnp.einsum(
        "skgj,sjke->skge", mixed_map, value_cache, preferred_element_type=jnp.float32
    )
    head_out = head_out + mixed_new[..., None] * value_new
    square_mean = jnp.mean(head_out * head_out, axis=-1, keepdims=True)
    normed = head_out * lax.rsqrt(square_mean + head_epsilon) * head_gain * head_scale
    return normed.astype(jnp.bfloat16).reshape(seq_count, kv_local * group_size * VD)


def on_device(
    tokens,
    query_weight,
    key_weight,
    value_weight,
    out_weight,
    head_lambda,
    head_gain,
    key_cache,
    value_cache,
    lengths,
    first_gain,
    second_gain,
    expert_ids,
    route_weights,
    expert_gate,
    expert_up,
    expert_down,
    dense_gate,
    dense_up,
    dense_down,
    dense_mix,
):
    seq_count = tokens.shape[0]
    model_width = tokens.shape[1]
    ep_count = lax.axis_size("ep")
    tp_count = lax.axis_size("tp")
    query_cols = query_weight.shape[1]
    key_cols = key_weight.shape[1]
    columns = lax.all_to_all(tokens, "ep", split_axis=1, concat_axis=0, tiled=True)
    summed = lax.psum_scatter(
        jnp.concatenate(
            [
                jnp.dot(columns, query_weight, preferred_element_type=jnp.float32),
                jnp.dot(columns, key_weight, preferred_element_type=jnp.float32),
                jnp.dot(columns, value_weight, preferred_element_type=jnp.float32),
            ],
            axis=1,
        ).astype(jnp.bfloat16),
        "ep",
        scatter_dimension=0,
        tiled=True,
    ).astype(jnp.float32)
    query_sum = summed[:, :query_cols]
    key_sum = summed[:, query_cols : query_cols + key_cols]
    value_sum = summed[:, query_cols + key_cols :]
    normed = attend(
        query_sum, key_sum, value_sum, head_lambda, head_gain, key_cache, value_cache, lengths
    )
    all_heads = lax.all_gather(normed, "ep", axis=0, tiled=True)
    column_part = jnp.dot(all_heads, out_weight, preferred_element_type=jnp.float32)
    column_part = lax.psum(column_part.astype(jnp.bfloat16), "tp").astype(jnp.float32)
    attention = lax.all_to_all(
        column_part.astype(jnp.bfloat16), "ep", split_axis=0, concat_axis=1, tiled=True
    )
    residual_in = residual_scale * tokens.astype(jnp.float32) + widened(attention)
    average = jnp.mean(residual_in, axis=-1, keepdims=True)
    centered = residual_in - average
    variance = jnp.mean(centered * centered, axis=-1, keepdims=True)
    hidden_in = (centered * lax.rsqrt(variance + layer_epsilon) * first_gain).astype(jnp.bfloat16)
    slice_width = model_width // tp_count
    own_cols = lax.dynamic_slice_in_dim(
        hidden_in, lax.axis_index("tp") * slice_width, slice_width, 1
    )
    flat_ids = expert_ids.reshape(-1)
    hit_table = (flat_ids[:, None] == jnp.arange(EXPERTS, dtype=jnp.int32)[None, :]).astype(
        jnp.int32
    )
    earlier = jnp.cumsum(hit_table, axis=0) - hit_table
    slot_index = jnp.sum(earlier * hit_table, axis=1)
    target = flat_ids * CAP + slot_index
    placed = jnp.arange(EXPERTS * CAP, dtype=jnp.int32)[:, None] == target[None, :]
    routed_rows = jnp.repeat(own_cols, TOPK, axis=0)
    packed = jnp.dot(placed.astype(jnp.bfloat16), routed_rows, preferred_element_type=jnp.float32)
    packed = packed.astype(jnp.bfloat16).reshape(ep_count, EXPERTS // ep_count, CAP, slice_width)
    arrived = lax.all_to_all(packed, "ep", split_axis=0, concat_axis=2, tiled=True)[0]
    expert_pre_gate = jnp.einsum(
        "erd,edf->erf", arrived, expert_gate, preferred_element_type=jnp.float32
    )
    expert_pre_up = jnp.einsum(
        "erd,edf->erf", arrived, expert_up, preferred_element_type=jnp.float32
    )
    all_rows = lax.all_gather(own_cols, "ep", axis=0, tiled=True)
    dense_pre_gate = jnp.dot(all_rows, dense_gate, preferred_element_type=jnp.float32)
    dense_pre_up = jnp.dot(all_rows, dense_up, preferred_element_type=jnp.float32)
    expert_pre_gate, expert_pre_up, dense_pre_gate, dense_pre_up = (
        lax.psum(expert_pre_gate.astype(jnp.bfloat16), "tp").astype(jnp.float32),
        lax.psum(expert_pre_up.astype(jnp.bfloat16), "tp").astype(jnp.float32),
        lax.psum(dense_pre_gate.astype(jnp.bfloat16), "tp").astype(jnp.float32),
        lax.psum(dense_pre_up.astype(jnp.bfloat16), "tp").astype(jnp.float32),
    )
    expert_hidden = (jax.nn.silu(expert_pre_gate) * expert_pre_up).astype(jnp.bfloat16)
    expert_result = jnp.einsum(
        "erf,efd->erd", expert_hidden, expert_down, preferred_element_type=jnp.float32
    )
    expert_result = expert_result.astype(jnp.bfloat16)
    local_experts = expert_result.shape[0]
    expert_result = expert_result.reshape(1, local_experts, ep_count, CAP, slice_width)
    returned = lax.all_to_all(expert_result, "ep", split_axis=2, concat_axis=0, tiled=True).reshape(
        EXPERTS * CAP, slice_width
    )
    route_gates = route_weights / jnp.sum(route_weights, axis=-1, keepdims=True)
    weighted = placed.astype(jnp.float32) * route_gates.reshape(-1)[None, :]
    combine_matrix = jnp.sum(weighted.T.reshape(seq_count, TOPK, EXPERTS * CAP), axis=1)
    expert_mix = jnp.dot(
        combine_matrix, returned.astype(jnp.float32), precision=lax.Precision.HIGHEST
    )
    dense_hidden = (jax.nn.silu(dense_pre_gate) * dense_pre_up).astype(jnp.bfloat16)
    dense_part = jnp.dot(dense_hidden, dense_down, preferred_element_type=jnp.float32)
    dense_out = widened(
        lax.psum_scatter(
            dense_part.astype(jnp.bfloat16), "ep", scatter_dimension=0, tiled=True
        ).astype(jnp.float32)
    )
    mix_gate = jax.nn.sigmoid(jnp.dot(hidden_in, dense_mix, preferred_element_type=jnp.float32))
    combined = (
        residual_scale * own_cols.astype(jnp.float32) + expert_mix + mix_gate[:, None] * dense_out
    )
    moments = lax.psum((jnp.sum(combined, axis=1), jnp.sum(combined * combined, axis=1)), "tp")
    average = moments[0] / model_width
    variance = moments[1] / model_width - average * average
    layer_out = (
        (combined - average[:, None]) * lax.rsqrt(variance + layer_epsilon)[:, None] * second_gain
    )
    return layer_out.astype(jnp.bfloat16)


def solution(mesh):
    return jax.shard_map(
        on_device,
        mesh=mesh,
        in_specs=(
            P("ep", None),
            P("ep", "tp"),
            P("ep", "tp"),
            P("ep", "tp"),
            P("tp", "ep"),
            P("tp"),
            P(),
            P("ep", None, "tp", None),
            P("ep", None, "tp", None),
            P("ep"),
            P(),
            P("tp"),
            P("ep", None),
            P("ep", None),
            P("ep", "tp", None),
            P("ep", "tp", None),
            P("ep", None, "tp"),
            P("tp", "ep"),
            P("tp", "ep"),
            P("ep", "tp"),
            P(),
        ),
        out_specs=P("ep", "tp"),
        check_vma=False,
    )
```

profile of v0, /device:TPU:0, one launch (start us, length us, event | category | flops | bytes accessed | tf_op | source)
XLA Modules:
  0.0 277.1 jit_solution(7512981496425636407)
XLA Ops:
  6.5 1.7 copy.150
  8.2 5.2 %all-to-all-start = ((bf16[16,4,1024]{2,0,1:T(8,128)(2,1)}), bf16[16,4,1024]{2,0,1:T(8,128)(2,1)S(1)}, u32[]{:S(2)}, u32[]{:S(2)}) async-start(bf16[16,4,1024]{2,0,1:T(8,128)(2,1)} %bitcast.102), calls=%async_computation | async-start | bytes 262144 | tf_op jit(solution)/shard_map/all_to_all | solution.py:113
  15.3 3.1 %all-to-all-done = bf16[16,4,1024]{2,0,1:T(8,128)(2,1)S(1)} async-done(((bf16[16,4,1024]{2,0,1:T(8,128)(2,1)}), bf16[16,4,1024]{2,0,1:T(8,128)(2,1)S(1)}, u32[]{:S(2)}, u32[]{:S(2)}) %all-to-all-start) | async-done | bytes 131104 | tf_op jit(solution)/shard_map/all_to_all | solution.py:113
  18.4 1.5 convolution_convert_fusion.3
  19.9 1.2 convolution_convert_fusion.10
  23.9 21.2 %copy.117 = bf16[16,1024,2,128]{1,3,2,0:T(8,128)(2,1)} copy(bf16[16,1024,2,128]{3,2,1,0:T(2,128)(2,1)} %param.28) | data formatting | bytes 16777216 | tf_op args[7]
  45.4 1.8 reduce-scatter.3.cloned.1.call-done
  49.6 4.8 %fusion.49 = (f32[16,2,2,2]{2,3,1,0:T(2,128)S(1)}, f32[16,2,2,2,1024]{4,2,3,1,0:T(2,128)S(1)}) fusion(bf16[16,1024,2,2,64]{1,4,3,2,0:T(8,128)(2,1)} %bitcast.103, bf16[16,2,2,2,32]{4,2,3,1,0:T(2,128)(2,1)S(1)} %get-tuple-element.14, bf16[16,2,2,2,32]{4,2,3,1,0:T(2,128)(2,1)S(1)} %get-tuple-element.13, pred[16,1024]{1,0:T(8,128)(4,1)S(1)} %iota_compare_fusion), kind=kOutput, calls=%fused_computation.101 | convolution fusion | flops 17203072 | bytes 8946176 | tf_op jit(solution)/shard_map/skgcd,sjkcd->skgcj/dot_general | solution.py:54
  56.0 4.9 %multiply_reduce_fusion.2 = (f32[16,2,2]{2,1,0:T(2,128)S(1)}, f32[16,2,2,128]{3,2,1,0:T(2,128)S(1)}) fusion(f32[16,2,128]{2,1,0:T(2,128)S(1)} %reshape.223, f32[16,2,2]{2,1,0:T(2,128)S(1)} %copy.122, bf16[16,1024,2,128]{3,2,1,0:T(2,128)(2,1)} %param.29, f32[16,2,2,2,1024]{4,2,3,1,0:T(2,128)S(1)} %fusion.17, f32[2,2]{1,0:T(2,128)S(1)} %mul.298), kind=kOutput, calls=%fused_computation.66 | convolution fusion | flops 17006528 | bytes 8962576 | tf_op jit(solution)/shard_map/skgj,sjke->skge/dot_general | solution.py:75
  61.2 8.2 %all_gather.6 = bf16[64,512]{1,0:T(8,128)(2,1)S(1)} all-gather(bf16[16,512]{1,0:T(8,128)(2,1)S(1)} %reshape.214), channel_id=1, replica_groups=mesh['ep'=4,'tp'=8] {'ep'}, dimensions={0}, use_global_device_ids=true | all-gather | bytes 81920 | tf_op jit(solution)/shard_map/all_gather | solution.py:133
  70.4 55.1 %all-reduce.5.cloned.1.call-done = bf16[4,16,1024]{2,1,0:T(8,128)(2,1)} async-done(((bf16[4,16,1024]{2,1,0:T(8,128)(2,1)}), bf16[4,16,1024]{2,1,0:T(8,128)(2,1)}) %all-reduce.5.cloned.1.call-update) | async-done | bytes 131088 | tf_op jit(solution)/shard_map/psum | solution.py:135
  125.5 3.6 %all-to-all-start.1 = ((bf16[4,16,1024]{2,1,0:T(8,128)(2,1)}), bf16[4,16,1024]{2,1,0:T(8,128)(2,1)S(1)}, u32[]{:S(2)}, u32[]{:S(2)}) async-start(bf16[4,16,1024]{2,1,0:T(8,128)(2,1)} %all-reduce.5.cloned.1.call-done), calls=%async_computation.2 | async-start | bytes 262144 | tf_op jit(solution)/shard_map/all_to_all | solution.py:136
  129.2 5.0 %all-to-all-done.1 = bf16[4,16,1024]{2,1,0:T(8,128)(2,1)S(1)} async-done(((bf16[4,16,1024]{2,1,0:T(8,128)(2,1)}), bf16[4,16,1024]{2,1,0:T(8,128)(2,1)S(1)}, u32[]{:S(2)}, u32[]{:S(2)}) %all-to-all-start.1) | async-done | bytes 131104 | tf_op jit(solution)/shard_map/all_to_all | solution.py:136
  134.8 7.6 %all_gather.7 = bf16[64,512]{1,0:T(8,128)(2,1)S(1)} all-gather(bf16[16,512]{1,0:T(8,128)(2,1)S(1)} %constant_dynamic-slice_fusion), channel_id=1, replica_groups=mesh['ep'=4,'tp'=8] {'ep'}, dimensions={0}, use_global_device_ids=true | all-gather | bytes 81920 | tf_op jit(solution)/shard_map/all_gather | solution.py:166
  143.2 3.3 %all-to-all-start.2 = ((bf16[4,4,4,512]{3,2,1,0:T(4,128)(2,1)}), bf16[4,4,4,512]{3,2,1,0:T(4,128)(2,1)S(1)}, u32[]{:S(2)}, u32[]{:S(2)}) async-start(bf16[4,4,4,512]{3,2,1,0:T(4,128)(2,1)} %reshape.216), calls=%async_computation.3 | async-start | bytes 131072 | tf_op jit(solution)/shard_map/all_to_all | solution.py:159
  148.3 3.1 %all-to-all-done.2 = bf16[4,4,4,512]{3,2,1,0:T(4,128)(2,1)S(1)} async-done(((bf16[4,4,4,512]{3,2,1,0:T(4,128)(2,1)}), bf16[4,4,4,512]{3,2,1,0:T(4,128)(2,1)S(1)}, u32[]{:S(2)}, u32[]{:S(2)}) %all-to-all-start.2) | async-done | bytes 65568 | tf_op jit(solution)/shard_map/all_to_all | solution.py:159
  151.4 5.3 %convolution_convert_fusion = bf16[4,16,2048]{2,1,0:T(8,128)(2,1)} fusion(bf16[4,16,512]{2,1,0:T(8,128)(2,1)S(1)} %squeeze.19, bf16[4,512,2048]{2,1,0:T(8,128)(2,1)} %param.36), kind=kOutput, calls=%fused_computation.2 | convolution fusion | flops 134348800 | bytes 8716288 | tf_op jit(solution)/shard_map/erd,edf->erf/dot_general | solution.py:163
  156.7 5.4 %convolution_convert_fusion.1 = bf16[4,16,2048]{2,1,0:T(8,128)(2,1)} fusion(bf16[4,16,512]{2,1,0:T(8,128)(2,1)S(1)} %squeeze.19, bf16[4,512,2048]{2,1,0:T(8,128)(2,1)} %param.35), kind=kOutput, calls=%fused_computation.3 | convolution fusion | flops 134348800 | bytes 8716288 | tf_op jit(solution)/shard_map/erd,edf->erf/dot_general | solution.py:160
  162.2 54.9 %all-reduce.7.cloned.1.call-done = (bf16[4,16,2048]{2,1,0:T(8,128)(2,1)}, bf16[4,16,2048]{2,1,0:T(8,128)(2,1)}, bf16[64,512]{1,0:T(8,128)(2,1)}, bf16[64,512]{1,0:T(8,128)(2,1)}) async-done(((bf16[4,16,2048]{2,1,0:T(8,128)(2,1)}, bf16[4,16,2048]{2,1,0:T(8,128)(2,1)}, bf16[64,512]{1,0:T(8,128)(2,1)}, bf16[64,512]{1,0:T(8,128)(2,1)}), (bf16[4,16,2048]{2,1,0:T(8,128)(2,1)}, bf16[4,16,2048]{2,1,0:T(8,128)(2,1)}, ...) | async-done | bytes 655376 | tf_op jit(solution)/shard_map/psum | solution.py:171
  217.1 4.8 %convolution_convert_fusion.7 = bf16[4,16,512]{2,1,0:T(8,128)(2,1)S(1)} fusion(bf16[4,2048,512]{2,1,0:T(8,128)(2,1)} %param.37, bf16[4,16,2048]{2,1,0:T(8,128)(2,1)} %get-tuple-element.9, bf16[4,16,2048]{2,1,0:T(8,128)(2,1)} %get-tuple-element.10), kind=kOutput, calls=%fused_computation.12 | convolution fusion | flops 135299072 | bytes 8978432 | tf_op jit(solution)/shard_map/erf,efd->erd/dot_general | solution.py:176
  222.5 3.6 %all-to-all-start.3 = ((bf16[1,4,4,4,512]{4,3,1,0,2:T(4,128)(2,1)}), bf16[1,4,4,4,512]{4,3,1,0,2:T(4,128)(2,1)S(1)}, u32[]{:S(2)}, u32[]{:S(2)}) async-start(bf16[1,4,4,4,512]{4,3,1,0,2:T(4,128)(2,1)} %copy.129), calls=%async_computation.4 | async-start | bytes 131072 | tf_op jit(solution)/shard_map/all_to_all | solution.py:182
  227.2 3.8 %all-to-all-done.3 = bf16[1,4,4,4,512]{4,3,1,0,2:T(4,128)(2,1)S(1)} async-done(((bf16[1,4,4,4,512]{4,3,1,0,2:T(4,128)(2,1)}), bf16[1,4,4,4,512]{4,3,1,0,2:T(4,128)(2,1)S(1)}, u32[]{:S(2)}, u32[]{:S(2)}) %all-to-all-start.3) | async-done | bytes 65568 | tf_op jit(solution)/shard_map/all_to_all | solution.py:182
  231.0 22.0 %reduce-scatter.5.cloned.1.call-done = bf16[16,512]{1,0:T(8,128)(2,1)} async-done(((bf16[64,512]{1,0:T(8,128)(2,1)}), bf16[16,512]{1,0:T(8,128)(2,1)}) %reduce-scatter.5.cloned.1.call-update) | async-done | bytes 16400 | tf_op jit(solution)/shard_map/reduce_scatter | solution.py:194
  254.1 15.8 %all-reduce = (f32[16]{0:T(128)S(1)}, f32[16]{0:T(128)S(1)}) all-reduce(f32[16]{0:T(128)S(1)} %get-tuple-element.6, f32[16]{0:T(128)S(1)} %get-tuple-element.5), channel_id=1, replica_groups=mesh['ep'=4,'tp'=8] {'tp'}, use_global_device_ids=true, to_apply=%region_19.20 | all-reduce | flops 32 | bytes 256 | tf_op jit(solution)/shard_map/psum | solution.py:202
  (104 shorter events, 16.8 us)
Async XLA Ops:
  6.5 62.9 %copy-start = (bf16[512,1024]{1,0:T(8,128)(2,1)S(1)}, bf16[512,1024]{1,0:T(8,128)(2,1)}, u32[]{:S(2)}) copy-start(bf16[512,1024]{1,0:T(8,128)(2,1)} %param.25) | copy-start | bytes 3145732
  8.2 10.2 %all-to-all-start = ((bf16[16,4,1024]{2,0,1:T(8,128)(2,1)}), bf16[16,4,1024]{2,0,1:T(8,128)(2,1)S(1)}, u32[]{:S(2)}, u32[]{:S(2)}) async-start(bf16[16,4,1024]{2,0,1:T(8,128)(2,1)} %bitcast.102), calls=%async_computation | async-start | bytes 262144 | tf_op jit(solution)/shard_map/all_to_all | solution.py:113
  13.4 33.8 %reduce-scatter.3.cloned.1.call-start = ((), (), s32[]{:S(2)}) async-start(), calls=%async_computation.6 | async-start | bytes 163840 | tf_op jit(solution)/shard_map/reduce_scatter | solution.py:114
  23.1 102.4 %all-reduce.5.cloned.1.call-start = ((), (), s32[]{:S(2)}) async-start(), calls=%async_computation.7 | async-start | bytes 262144 | tf_op jit(solution)/shard_map/psum | solution.py:135
  23.9 21.2 %copy-start.13 = (f32[4]{0:T(128)S(1)}, f32[4]{0:T(128)}, u32[]{:S(2)}) copy-start(f32[4]{0:T(128)} %param.26) | copy-start | bytes 52
  54.3 6.7 %copy-start.9 = (f32[128]{0:T(128)S(1)}, f32[128]{0:T(128)}, u32[]{:S(2)}) copy-start(f32[128]{0:T(128)} %param.27) | copy-start | bytes 1540
  54.3 16.0 %copy-start.6 = (s32[16,2]{0,1:T(2,128)S(1)}, s32[16,2]{0,1:T(2,128)}, u32[]{:S(2)}) copy-start(s32[16,2]{0,1:T(2,128)} %param.33) | copy-start | bytes 388
  54.4 74.8 %copy-start.5 = (bf16[4096]{0:T(1024)(128)(2,1)S(1)}, bf16[4096]{0:T(1024)(128)(2,1)}, u32[]{:S(2)}) copy-start(bf16[4096]{0:T(1024)(128)(2,1)} %param.41) | copy-start | bytes 24580
  54.4 74.8 %copy-start.7 = (f32[16,2]{0,1:T(2,128)S(1)}, f32[16,2]{0,1:T(2,128)}, u32[]{:S(2)}) copy-start(f32[16,2]{0,1:T(2,128)} %param.34) | copy-start | bytes 388
  54.4 79.8 %copy-start.1 = (bf16[16,4096]{1,0:T(8,128)(2,1)S(1)}, bf16[16,4096]{1,0:T(8,128)(2,1)}, u32[]{:S(2)}) copy-start(bf16[16,4096]{1,0:T(8,128)(2,1)} %param.21) | copy-start | bytes 393220
  54.4 80.2 %copy-start.4 = (f32[4096]{0:T(1024)S(1)}, f32[4096]{0:T(1024)}, u32[]{:S(2)}) copy-start(f32[4096]{0:T(1024)} %param.31) | copy-start | bytes 49156
  54.4 92.2 %copy-start.2 = (bf16[512,512]{1,0:T(8,128)(2,1)S(1)}, bf16[512,512]{1,0:T(8,128)(2,1)}, u32[]{:S(2)}) copy-start(bf16[512,512]{1,0:T(8,128)(2,1)} %param.39) | copy-start | bytes 1572868
  54.4 93.0 %copy-start.3 = (bf16[512,512]{1,0:T(8,128)(2,1)S(1)}, bf16[512,512]{1,0:T(8,128)(2,1)}, u32[]{:S(2)}) copy-start(bf16[512,512]{1,0:T(8,128)(2,1)} %param.38) | copy-start | bytes 1572868
  125.5 8.7 %all-to-all-start.1 = ((bf16[4,16,1024]{2,1,0:T(8,128)(2,1)}), bf16[4,16,1024]{2,1,0:T(8,128)(2,1)S(1)}, u32[]{:S(2)}, u32[]{:S(2)}) async-start(bf16[4,16,1024]{2,1,0:T(8,128)(2,1)} %all-reduce.5.cloned.1.call-done), calls=%async_computation.2 | async-start | bytes 262144 | tf_op jit(solution)/shard_map/all_to_all | solution.py:136
  143.2 8.1 %all-to-all-start.2 = ((bf16[4,4,4,512]{3,2,1,0:T(4,128)(2,1)}), bf16[4,4,4,512]{3,2,1,0:T(4,128)(2,1)S(1)}, u32[]{:S(2)}, u32[]{:S(2)}) async-start(bf16[4,4,4,512]{3,2,1,0:T(4,128)(2,1)} %reshape.216), calls=%async_computation.3 | async-start | bytes 131072 | tf_op jit(solution)/shard_map/all_to_all | solution.py:159
  146.5 70.5 %all-reduce.7.cloned.1.call-start = ((), (), s32[]{:S(2)}) async-start(), calls=%async_computation.9 | async-start | bytes 1310720 | tf_op jit(solution)/shard_map/psum | solution.py:171
  156.7 69.5 %copy-start.10 = (bf16[512,512]{1,0:T(8,128)(2,1)S(1)}, bf16[512,512]{1,0:T(8,128)(2,1)}, u32[]{:S(2)}) copy-start(bf16[512,512]{1,0:T(8,128)(2,1)} %param.40) | copy-start | bytes 1572868
  156.7 113.2 %copy-start.8 = (f32[512]{0:T(512)S(1)}, f32[512]{0:T(512)}, u32[]{:S(2)}) copy-start(f32[512]{0:T(512)} %param.32) | copy-start | bytes 6148
  217.1 9.1 %copy-start.11 = (bf16[64,512]{1,0:T(8,128)(2,1)S(1)}, bf16[64,512]{1,0:T(8,128)(2,1)}, u32[]{:S(2)}) copy-start(bf16[64,512]{1,0:T(8,128)(2,1)} %get-tuple-element.11) | copy-start | bytes 196612
  217.1 9.1 %copy-start.12 = (bf16[64,512]{1,0:T(8,128)(2,1)S(1)}, bf16[64,512]{1,0:T(8,128)(2,1)}, u32[]{:S(2)}) copy-start(bf16[64,512]{1,0:T(8,128)(2,1)} %get-tuple-element.12) | copy-start | bytes 196612
  222.5 8.5 %all-to-all-start.3 = ((bf16[1,4,4,4,512]{4,3,1,0,2:T(4,128)(2,1)}), bf16[1,4,4,4,512]{4,3,1,0,2:T(4,128)(2,1)S(1)}, u32[]{:S(2)}, u32[]{:S(2)}) async-start(bf16[1,4,4,4,512]{4,3,1,0,2:T(4,128)(2,1)} %copy.129), calls=%async_computation.4 | async-start | bytes 131072 | tf_op jit(solution)/shard_map/all_to_all | solution.py:182
  226.2 26.9 %reduce-scatter.5.cloned.1.call-start = ((), (), s32[]{:S(2)}) async-start(), calls=%async_computation.8 | async-start | bytes 81920 | tf_op jit(solution)/shard_map/reduce_scatter | solution.py:194
Sparse Core Ops, SparseCore 0:
  23.3 23.8 reduce-scatter.2
  70.5 54.9 all-reduce.4
  162.2 54.8 all-reduce.6
  229.4 23.6 reduce-scatter.4
where the time goes:
time: 279 us; the launch traced here: 277 us
  waiting for transfers between devices  149 us (53%)
  matrix products  34 us (12%)
  blocking collectives  31.6 us (11%)
  local copies, waits for them, and re-layouts  27.8 us (10%)
  starting transfers between devices  15.9 us (6%)
  between operations  13.5 us (5%)
  other arithmetic  5.45 us (2%)
    psum x1, waiting for transfers between devices, on_device(): lax.psum(column_part.astype(jnp.bfloat16), 'tp').astype(jnp.float32)  55.1 us
    psum x1, waiting for transfers between devices, on_device(): lax.psum(expert_pre_up.astype(jnp.bfloat16), 'tp').astype(jnp.float32)  54.9 us
    reduce_scatter x1, waiting for transfers between devices, on_device(): lax.psum_scatter(dense_part.astype(jnp.bfloat16), 'ep', scatter_dimension...  22 us
    unnamed x31, local copies, waits for them, and re-layouts  22 us
    psum x1, blocking collectives, on_device(): lax.psum((jnp.sum(combined, axis=1), jnp.sum(combined * combined, axis=1)...  15.8 us
    all_gather x1, blocking collectives, on_device(): all_heads = lax.all_gather(normed, 'ep', axis=0, tiled=True)  8.17 us
    all_gather x1, blocking collectives, on_device(): all_rows = lax.all_gather(own_cols, 'ep', axis=0, tiled=True)  7.64 us
  transfers between devices with their start and end apart: 8, of which 8 were waited for; matrix products, arithmetic and copies ran while one was open for 10% of the time, Pallas kernels for 0%

commit v1 on v0

v1 whole, which is shorter than its diff:
```python
import functools

import jax
import jax.numpy as jnp
from jax import lax
from jax.experimental import pallas as pl
from jax.experimental.pallas import tpu as pltpu
from jax.sharding import PartitionSpec as P

SUB = 64
EXPERTS = 16
TOPK = 2
CAP = 4
PAD = 16
LANES = 128

theta_base = 500000.0
score_scale = 0.125
head_scale = 0.8
residual_scale = 2.0**0.5
layer_epsilon = 1e-05
head_epsilon = 1e-06
F32 = jnp.float32
BF16 = jnp.bfloat16
MESH = pl.DeviceIdType.MESH


def mm(a, b):
    return lax.dot_general(a, b, (((1,), (0,)), ((), ())), preferred_element_type=F32)


def aligned(index, size):
    return pl.ds(pl.multiple_of(index * size, LANES), size)


def kernel(
    ep, tp, kv, heads,
    tok, cosr, sinr, lens, lam, hgain, fgain, sgain, ids, rw, dmix,
    qw, kw, vw, ow, kc, vc, eg, eu, ed, dg, du, dd,
    out,
    wq, wk, wv, wo, kbuf, vbuf, weg, weu, wed, wdg, wdu, wdd,
    cols, sB, rB, qs, ks, vs, hn, heads_all, sD, rD, stat, mixp, sE, rE, arr,
    sF, rF, sFd, rFd, hG, hGd, acc, sH, rH, mom,
    wsem, ksem, vsem, esem, ssem, rsem, sdsem, rdsem,
):
    me = lax.axis_index("ep")
    mt = lax.axis_index("tp")
    seqs = tok.shape[0]
    cdim = qw.shape[0]
    qc, kcn = qw.shape[1], kw.shape[1]
    own = ed.shape[2]
    width = tok.shape[1]
    ratio = tp // ep
    le = eg.shape[0]
    slots = ep * CAP
    fc = eg.shape[2] // tp
    fd = dg.shape[1]
    nrow = 2 * heads

    def load(src, dst, sem):
        cp = pltpu.make_async_copy(src, dst, sem)
        cp.start()
        return cp

    cq = load(qw, wq, wsem.at[0])
    ck = load(kw, wk, wsem.at[1])
    cv = load(vw, wv, wsem.at[2])

    sends = []

    def post(phase, axis, src, dst):
        n, mine = (ep, me) if axis == "ep" else (tp, mt)
        copies = []
        for k in range(1, n):
            peer = lax.rem(mine + k, n)
            where = (peer, mt) if axis == "ep" else (me, peer)
            cp = pltpu.make_async_remote_copy(
                src_ref=src(peer), dst_ref=dst(mine),
                send_sem=ssem.at[phase, k], recv_sem=rsem.at[phase, k],
                device_id=where, device_id_type=MESH,
            )
            cp.start()
            copies.append(cp)
        sends.extend(copies)
        return copies

    def arrive(copies):
        for cp in copies:
            cp.wait_recv()

    got = post(0, "ep", lambda p: tok.at[:, aligned(p, cdim)], lambda m: cols.at[m])
    cols[me] = tok[:, aligned(me, cdim)]

    kcp = [load(kc.at[s], kbuf.at[s], ksem.at[s]) for s in range(seqs)]
    vcp = [load(vc.at[s], vbuf.at[s], vsem.at[s]) for s in range(seqs)]
    co = load(ow, wo, wsem.at[3])
    cdg = load(dg, wdg, wsem.at[4])
    cdu = load(du, wdu, wsem.at[5])
    cdd = load(dd, wdd, wsem.at[6])
    ecp = []
    for e in range(le):
        ecp.append(load(eg.at[e], weg.at[e], esem.at[0, e]))
        ecp.append(load(eu.at[e], weu.at[e], esem.at[1, e]))
    edc = [load(ed.at[e], wed.at[e], esem.at[2, e]) for e in range(le)]

    lane = lax.broadcasted_iota(jnp.int32, (seqs, LANES), 1)
    idv = [ids[:, k : k + 1] for k in range(TOPK)]
    hit = [(lane == i).astype(F32) for i in idv]
    low = (
        lax.broadcasted_iota(jnp.int32, (seqs, seqs), 1)
        < lax.broadcasted_iota(jnp.int32, (seqs, seqs), 0)
    ).astype(BF16)
    earlier = mm(low, (hit[0] + hit[1]).astype(BF16))
    rsum = rw[:, 0:1] + rw[:, 1:2]
    slot_lane = lax.broadcasted_iota(jnp.int32, (seqs, ep * PAD), 1)
    place = jnp.zeros((seqs, ep * PAD), F32)
    mixw = jnp.zeros((seqs, ep * PAD), F32)
    for k in range(TOPK):
        slot = jnp.sum(earlier * hit[k], axis=1, keepdims=True).astype(jnp.int32)
        home = jnp.zeros_like(idv[k])
        for p in range(1, ep):
            home = home + (idv[k] >= p * le).astype(jnp.int32)
        col = home * PAD + (idv[k] - home * le) * CAP + slot
        eq = (slot_lane == col).astype(F32)
        place = place + eq
        mixw = mixw + eq * (rw[:, k : k + 1] / rsum)

    cq.wait()
    ck.wait()
    cv.wait()
    arrive(got)
    x = cols[...].reshape(ep * seqs, cdim)
    sB[:, :, 0:qc] = mm(x, wq[...]).astype(BF16).reshape(ep, seqs, qc)
    sB[:, :, qc : qc + kcn] = mm(x, wk[...]).astype(BF16).reshape(ep, seqs, kcn)
    sB[:, :, qc + kcn :] = mm(x, wv[...]).astype(BF16).reshape(ep, seqs, kcn)
    got = post(1, "ep", lambda p: sB.at[p], lambda m: rB.at[m])
    rB[me] = sB[me]
    arrive(got)
    total = rB[0].astype(F32)
    for p in range(1, ep):
        total = total + rB[p].astype(F32)
    total = total.astype(BF16).astype(F32)

    lane = lax.broadcasted_iota(jnp.int32, (seqs, LANES), 1)
    lower = (lane & (SUB - 1)) < SUB // 2
    first = lane < SUB
    cosine, sine = cosr[...], sinr[...]

    def turned(v):
        up = pltpu.roll(v, LANES - SUB // 2, 1)
        down = pltpu.roll(v, SUB // 2, 1)
        return (v * cosine + jnp.where(lower, up, down) * sine).astype(BF16).astype(F32)

    group = heads // kv
    for k in range(kv):
        krot = turned(total[:, qc + k * LANES : qc + (k + 1) * LANES])
        vnew = total[:, qc + kcn + k * LANES : qc + kcn + (k + 1) * LANES]
        for g in range(group):
            h = k * group + g
            q = turned(total[:, h * LANES : (h + 1) * LANES])
            qs[:, h, :] = jnp.where(first, q, 0.0)
            qs[:, heads + h, :] = jnp.where(first, 0.0, q)
            ks[:, h, :] = krot
            ks[:, heads + h, :] = krot
            vs[:, h, :] = vnew

    npos = kbuf.shape[1]
    ccol = lax.broadcasted_iota(jnp.int32, (nrow, npos), 1)
    crow = lax.broadcasted_iota(jnp.int32, (nrow, npos), 0)
    krow = jnp.zeros_like(crow)
    for r in range(nrow):
        krow = jnp.where(crow == r, (r % heads) // group, krow)
    mine = lax.rem(ccol, kv) == krow if kv > 1 else ccol >= 0
    lamc = lam[...]
    gain = hgain[...] * head_scale

    def one(s):
        q8 = qs[s]
        score = lax.dot_general(
            q8.astype(BF16), kbuf[s], (((1,), (1,)), ((), ())), preferred_element_type=F32
        )
        score = jnp.where(mine & (ccol < lens[s] * kv), score * score_scale, -1e30)
        fresh = jnp.sum(q8 * ks[s], axis=1, keepdims=True) * score_scale
        high = jnp.maximum(jnp.max(score, axis=1, keepdims=True), fresh)
        ex = jnp.exp(score - high)
        fx = jnp.exp(fresh - high)
        inv = 1.0 / (jnp.sum(ex, axis=1, keepdims=True) + fx)
        pr = ex * inv
        fp = fx * inv
        dmap = (pr[0:heads] - lamc * pr[heads:nrow]).astype(BF16)
        dnew = (fp[0:heads] - lamc * fp[heads:nrow]).astype(BF16).astype(F32)
        ho = mm(dmap, vbuf[s]) + dnew * vs[s]
        sq = jnp.mean(ho * ho, axis=1, keepdims=True)
        hn[s] = ho * lax.rsqrt(sq + head_epsilon) * gain

    step = 4

    def some(i, carry):
        for u in range(step):
            s = i * step + u
            pltpu.make_async_copy(kc.at[s], kbuf.at[s], ksem.at[s]).wait()
            pltpu.make_async_copy(vc.at[s], vbuf.at[s], vsem.at[s]).wait()
        for u in range(step):
            one(i * step + u)
        return carry

    lax.fori_loop(0, seqs // step, some, 0)
    for h in range(heads):
        heads_all[me, :, h * LANES : (h + 1) * LANES] = hn[:, h, :].astype(BF16)
    got = post(2, "ep", lambda p: heads_all.at[me], lambda m: heads_all.at[m])
    co.wait()
    arrive(got)
    part = mm(heads_all[...].reshape(ep * seqs, heads * LANES), wo[...])
    for h in range(ratio):
        sD[h] = part[:, h * own : (h + 1) * own].astype(BF16).reshape(ep, seqs, own)

    def dcopy(ds, h):
        s = lax.rem(me + ds, ep)
        t = me * ratio + h
        return t, pltpu.make_async_remote_copy(
            src_ref=sD.at[h, s], dst_ref=rD.at[mt],
            send_sem=sdsem.at[ds, h], recv_sem=rdsem.at[mt],
            device_id=(s, t), device_id_type=MESH,
        )

    for ds in range(ep):
        for h in range(ratio):
            t, cp = dcopy(ds, h)
            if ds == 0:
                @pl.when(t == mt)
                def _():
                    pltpu.make_async_copy(sD.at[h, me], rD.at[mt], rdsem.at[mt]).start()

                @pl.when(t != mt)
                def _():
                    cp.start()
            else:
                cp.start()
    for t in range(tp):
        pltpu.make_async_copy(rD.at[t], rD.at[t], rdsem.at[t]).wait()
    attn = rD[0].astype(F32)
    for t in range(1, tp):
        attn = attn + rD[t].astype(F32)
    attn = attn.astype(BF16).astype(F32)
    resid = residual_scale * tok[:, aligned(mt, own)].astype(F32) + attn
    mloc = jnp.mean(resid, axis=1, keepdims=True)
    cent = resid - mloc
    m2 = jnp.sum(cent * cent, axis=1, keepdims=True)
    stat[mt] = jnp.where(lane == 0, mloc, m2)
    got = post(3, "tp", lambda p: stat.at[mt], lambda m: stat.at[m])
    arrive(got)
    mean = stat[0]
    for t in range(1, tp):
        mean = mean + stat[t]
    sqs = mean[:, 1:2]
    mean = mean[:, 0:1] * (1.0 / tp)
    for t in range(tp):
        d = stat[t][:, 0:1] - mean
        sqs = sqs + d * d * own
    rstd = lax.rsqrt(sqs * (1.0 / width) + layer_epsilon)
    hidden = ((resid - mean) * rstd * fgain[:, aligned(mt, own)]).astype(BF16)
    hidf = hidden.astype(F32)
    dotp = jnp.sum(hidf * dmix[:, aligned(mt, own)], axis=1, keepdims=True)

    packed = lax.dot_general(
        place, hidf, (((0,), (0,)), ((), ())), preferred_element_type=F32
    ).astype(BF16)
    for p in range(ep):
        sE[p, 0:seqs] = hidden
        sE[p, seqs : seqs + PAD] = packed[p * PAD : (p + 1) * PAD]
    got = post(4, "ep", lambda p: sE.at[p], lambda m: rE.at[m])
    mixp[mt] = jnp.broadcast_to(dotp, (seqs, LANES))
    got_mix = post(5, "tp", lambda p: mixp.at[mt], lambda m: mixp.at[m])
    rE[me] = sE[me]
    nslot = le * slots
    prow = lax.broadcasted_iota(jnp.int32, (nslot, ep * PAD), 0)
    pcol = lax.broadcasted_iota(jnp.int32, (nslot, ep * PAD), 1)
    pe, ps, pc = prow // slots, (prow % slots) // CAP, prow % CAP
    perm = (pcol == ps * PAD + pe * CAP + pc).astype(BF16)
    arrive(got)
    rows = rE[:, 0:seqs].reshape(ep * seqs, own)
    routed = rE[:, seqs : seqs + PAD].reshape(ep * PAD, own)
    arr[...] = mm(perm, routed).astype(BF16)

    cdg.wait()
    cdu.wait()
    sFd[:, :, 0:fd] = mm(rows, wdg[...]).reshape(tp, ep * seqs // tp, fd).astype(BF16)
    sFd[:, :, fd:] = mm(rows, wdu[...]).reshape(tp, ep * seqs // tp, fd).astype(BF16)
    got_d = post(6, "tp", lambda p: sFd.at[p], lambda m: rFd.at[m])
    rFd[mt] = sFd[mt]
    for cp in ecp:
        cp.wait()

    def fcopy(k):
        peer = lax.rem(mt + k, tp)
        return pltpu.make_async_remote_copy(
            src_ref=sF.at[peer], dst_ref=rF.at[mt],
            send_sem=ssem.at[7, k], recv_sem=rsem.at[7, k],
            device_id=(me, peer), device_id_type=MESH,
        )

    def chunk(peer, into):
        for e in range(le):
            xe = arr[e * slots : (e + 1) * slots]
            into[peer, 0, e * slots : (e + 1) * slots] = mm(
                xe, weg[e, :, aligned(peer, fc)]
            ).astype(BF16)
            into[peer, 1, e * slots : (e + 1) * slots] = mm(
                xe, weu[e, :, aligned(peer, fc)]
            ).astype(BF16)

    def fstep(k, carry):
        chunk(lax.rem(mt + k, tp), sF)
        fcopy(k).start()
        return carry

    lax.fori_loop(1, tp, fstep, 0)
    chunk(mt, rF)

    arrive(got_d)
    dsum = rFd[0].astype(F32)
    for t in range(1, tp):
        dsum = dsum + rFd[t].astype(F32)
    dg_, du_ = dsum[:, 0:fd], dsum[:, fd:]
    hGd[mt] = (dg_ / (1.0 + jnp.exp(-dg_)) * du_).astype(BF16)
    got_d = post(8, "tp", lambda p: hGd.at[mt], lambda m: hGd.at[m])

    for k in range(1, tp):
        fcopy(k).wait_recv()
    gs, us = rF[0, 0].astype(F32), rF[0, 1].astype(F32)
    for t in range(1, tp):
        gs = gs + rF[t, 0].astype(F32)
        us = us + rF[t, 1].astype(F32)
    hG[mt] = (gs / (1.0 + jnp.exp(-gs)) * us).astype(BF16)
    got = post(9, "tp", lambda p: hG.at[mt], lambda m: hG.at[m])

    cdd.wait()
    arrive(got_d)
    dh = hGd[...].astype(F32).reshape(ep * seqs, fd).astype(BF16)
    sH[:, PAD : PAD + seqs] = mm(dh, wdd[...]).astype(BF16).reshape(ep, seqs, own)
    for cp in edc:
        cp.wait()

    def down(src):
        for e in range(le):
            acc[e] += mm(hG[src, e * slots : (e + 1) * slots], wed[e, aligned(src, fc), :])

    acc[...] = jnp.zeros_like(acc)
    down(mt)
    for k in range(1, tp):
        got[k - 1].wait_recv()
        down(lax.rem(mt + tp - k, tp))
    res = acc[...].reshape(nslot, own).astype(BF16)
    back = lax.dot_general(
        perm, res, (((0,), (0,)), ((), ())), preferred_element_type=F32
    ).astype(BF16)
    sH[:, 0:PAD] = back.reshape(ep, PAD, own)
    got = post(10, "ep", lambda p: sH.at[p], lambda m: rH.at[m])
    rH[me] = sH[me]
    arrive(got_mix)
    mixs = mixp[0]
    for t in range(1, tp):
        mixs = mixs + mixp[t]
    gate = 1.0 / (1.0 + jnp.exp(-mixs[:, 0:1]))
    arrive(got)
    returned = rH[:, 0:PAD].reshape(ep * PAD, own)
    hi = mixw.astype(BF16)
    rest = mixw - hi.astype(F32)
    mid = rest.astype(BF16)
    last = (rest - mid.astype(F32)).astype(BF16)
    emix = mm(hi, returned) + mm(mid, returned) + mm(last, returned)
    dout = rH[0, PAD : PAD + seqs].astype(F32)
    for p in range(1, ep):
        dout = dout + rH[p, PAD : PAD + seqs].astype(F32)
    dout = dout.astype(BF16).astype(F32)
    comb = residual_scale * hidf + emix + gate * dout
    s1 = jnp.sum(comb, axis=1, keepdims=True)
    s2 = jnp.sum(comb * comb, axis=1, keepdims=True)
    mom[mt] = jnp.where(lane == 0, s1, s2)
    got = post(11, "tp", lambda p: mom.at[mt], lambda m: mom.at[m])
    arrive(got)
    ms = mom[0]
    for t in range(1, tp):
        ms = ms + mom[t]
    ms = ms * (1.0 / width)
    avg = ms[:, 0:1]
    var = ms[:, 1:2] - avg * avg
    out[...] = ((comb - avg) * lax.rsqrt(var + layer_epsilon) * sgain[...]).astype(BF16)

    for cp in sends:
        cp.wait_send()
    for k in range(1, tp):
        fcopy(k).wait_send()
    for ds in range(ep):
        for h in range(ratio):
            t, cp = dcopy(ds, h)
            if ds == 0:
                @pl.when(t != mt)
                def _():
                    cp.wait_send()
            else:
                cp.wait_send()


PHASES = 12


def on_device(
    tokens, query_weight, key_weight, value_weight, out_weight, head_lambda, head_gain,
    key_cache, value_cache, lengths, first_gain, second_gain, expert_ids, route_weights,
    expert_gate, expert_up, expert_down, dense_gate, dense_up, dense_down, dense_mix,
):
    ep, tp = lax.axis_size("ep"), lax.axis_size("tp")
    seqs, width = tokens.shape
    cache, kv, vd = key_cache.shape[1:]
    heads = head_lambda.shape[0]
    cdim, qc = query_weight.shape
    kcn = key_weight.shape[1]
    le, own, ffe = expert_gate.shape
    fd = dense_gate.shape[1]
    fc = ffe // tp
    ratio = tp // ep
    slots = ep * CAP
    rows = ep * seqs
    npos = cache * kv
    lanes = jnp.arange(LANES, dtype=jnp.int32)
    half = SUB // 2
    frequency = theta_base ** (-((lanes % half).astype(F32) * (2.0 / SUB)))
    angles = lengths.astype(F32)[:, None] * frequency[None, :]
    sign = jnp.where(lanes % SUB < half, -1.0, 1.0)
    cosine = jnp.cos(angles)
    sine = jnp.sin(angles) * sign[None, :]
    vm = pl.BlockSpec(memory_space=pltpu.VMEM)
    sm = pl.BlockSpec(memory_space=pltpu.SMEM)
    hb = pl.BlockSpec(memory_space=pl.ANY)
    V = pltpu.VMEM
    D = pltpu.SemaphoreType.DMA
    n = max(ep, tp)
    return pl.pallas_call(
        functools.partial(kernel, ep, tp, kv, heads),
        out_shape=jax.ShapeDtypeStruct((seqs, own), BF16),
        in_specs=[vm] * 3 + [sm] + [vm] * 7 + [hb] * 12,
        out_specs=vm,
        scratch_shapes=[
            V(query_weight.shape, BF16), V(key_weight.shape, BF16), V(value_weight.shape, BF16),
            V(out_weight.shape, BF16),
            V((seqs, npos, vd), BF16), V((seqs, npos, vd), BF16),
            V(expert_gate.shape, BF16), V(expert_up.shape, BF16), V(expert_down.shape, BF16),
            V(dense_gate.shape, BF16), V(dense_up.shape, BF16), V(dense_down.shape, BF16),
            V((ep, seqs, cdim), BF16),
            V((ep, seqs, qc + 2 * kcn), BF16), V((ep, seqs, qc + 2 * kcn), BF16),
            V((seqs, 2 * heads, LANES), F32), V((seqs, 2 * heads, LANES), F32),
            V((seqs, heads, LANES), F32), V((seqs, heads, LANES), F32),
            V((ep, seqs, heads * LANES), BF16),
            V((ratio, ep, seqs, own), BF16), V((tp, seqs, own), BF16),
            V((tp, seqs, LANES), F32), V((tp, seqs, LANES), F32),
            V((ep, seqs + PAD, own), BF16), V((ep, seqs + PAD, own), BF16),
            V((le * slots, own), BF16),
            V((tp, 2, le * slots, fc), BF16), V((tp, 2, le * slots, fc), BF16),
            V((tp, rows // tp, 2 * fd), BF16), V((tp, rows // tp, 2 * fd), BF16),
            V((tp, le * slots, fc), BF16), V((tp, rows // tp, fd), BF16),
            V((le, slots, own), F32),
            V((ep, PAD + seqs, own), BF16), V((ep, PAD + seqs, own), BF16),
            V((tp, seqs, LANES), F32),
            D((7,)), D((seqs,)), D((seqs,)), D((3, le)),
            D((PHASES, n)), D((PHASES, n)), D((ep, ratio)), D((tp,)),
        ],
        compiler_params=pltpu.CompilerParams(
            has_side_effects=True, vmem_limit_bytes=62 * 1024 * 1024
        ),
        name="layer",
    )(
        tokens, cosine, sine, lengths, head_lambda.reshape(heads, 1), head_gain.reshape(1, -1),
        first_gain.reshape(1, -1), second_gain.reshape(1, -1), expert_ids, route_weights,
        dense_mix.astype(F32).reshape(1, -1),
        query_weight, key_weight, value_weight, out_weight,
        key_cache.reshape(seqs, npos, vd), value_cache.reshape(seqs, npos, vd),
        expert_gate, expert_up, expert_down, dense_gate, dense_up, dense_down,
    )


def solution(mesh):
    return jax.shard_map(
        on_device,
        mesh=mesh,
        in_specs=(
            P("ep", None), P("ep", "tp"), P("ep", "tp"), P("ep", "tp"), P("tp", "ep"),
            P("tp"), P(), P("ep", None, "tp", None), P("ep", None, "tp", None), P("ep"),
            P(), P("tp"), P("ep", None), P("ep", None), P("ep", "tp", None),
            P("ep", "tp", None), P("ep", None, "tp"), P("tp", "ep"), P("tp", "ep"),
            P("ep", "tp"), P(),
        ),
        out_specs=P("ep", "tp"),
        check_vma=False,
    )
```

time: 279 us -> 89.8 us (0.32)
  waiting for transfers between devices: 149 us -> 0 us
  Pallas kernels: 0 us -> 81.4 us
  matrix products: 34 us -> 0 us
  blocking collectives: 31.6 us -> 0 us
  local copies, waits for them, and re-layouts: 27.8 us -> 5.36 us
  starting transfers between devices: 15.9 us -> 0 us
  between operations: 13.5 us -> 0.01 us
    psum x2 -> x0, waiting for transfers between devices: 110 us -> none  [the longest x1 55.1 us: on_device(): lax.psum(column_part.astype(jnp.bfloat16), 'tp').astype(jnp.float32)]
    pallas_call x0 -> x1, Pallas kernels: none -> 81.4 us  [on_device(): pl.pallas_call(functools.partial(kernel, ep, tp, kv, heads), out_shape=ja...]
    dot_general x16 -> x0, matrix products: 34 us -> none  [the longest x1 5.35 us: on_device(): jnp.einsum('erd,edf->erf', arrived, expert_gate, preferred_element_type=j...]
    reduce_scatter x2 -> x0, waiting for transfers between devices: 23.8 us -> none  [the longest x1 22 us: on_device(): lax.psum_scatter(dense_part.astype(jnp.bfloat16), 'ep', scatter_dimension...]
    unnamed x31 -> x3, local copies, waits for them, and re-layouts: 22 us -> 4.02 us
    all_gather x2 -> x0, blocking collectives: 15.8 us -> none  [the longest x1 8.17 us: on_device(): all_heads = lax.all_gather(normed, 'ep', axis=0, tiled=True)]
    psum x1 -> x0, blocking collectives: 15.8 us -> none  [on_device(): lax.psum((jnp.sum(combined, axis=1), jnp.sum(combined * combined, axis=1)...]
    all_to_all x4 -> x0, starting transfers between devices: 15.8 us -> none  [the longest x1 5.19 us: on_device(): lax.all_to_all(tokens, 'ep', split_axis=1, concat_axis=0, tiled=True)]
  transfers between devices with their start and end apart: 8 -> 0, of which waited for: 8 -> 0; matrix products, arithmetic and copies ran while one was open for 10% -> 0% of each run, Pallas kernels for 0% -> 0%
where the time goes in v1:
time: 89.8 us; the launch traced here: 89.4 us
  Pallas kernels  81.4 us (91%)
  local copies, waits for them, and re-layouts  5.36 us (6%)
  other arithmetic  2.69 us (3%)
    pallas_call x1, Pallas kernels, on_device(): pl.pallas_call(functools.partial(kernel, ep, tp, kv, heads), out_shape=ja...  81.4 us
    unnamed x3, local copies, waits for them, and re-layouts  4.02 us

profile of v1, /device:TPU:0, one launch (start us, length us, event | category | flops | bytes accessed | tf_op | source)
XLA Modules:
  0.0 89.4 jit_solution(7505065375988305598)
XLA Ops:
  0.0 0.7 convert_element_type.11
  0.7 1.3 %copy.22.lam = f32[4,1]{1,0:T(4,128)} copy(f32[4,1]{0,1:T(1,128)} %bitcast.13) | data formatting | bytes 32 | tf_op jit(solution)/shard_map/reshape | solution.py:473
  2.0 1.4 %copy.23.ids = s32[16,2]{1,0:T(8,128)} copy(s32[16,2]{0,1:T(2,128)} %param.33) | data formatting | bytes 256 | tf_op args[12]
  3.4 1.3 %copy.24.rw = f32[16,2]{1,0:T(8,128)} copy(f32[16,2]{0,1:T(2,128)} %param.34) | data formatting | bytes 256 | tf_op args[13]
  4.7 0.7 fusion
  5.4 1.3 %reshape.56 = f32[4096]{0:T(1024)} convert(bf16[4096]{0:T(1024)(128)(2,1)} %param.41) | non-fusion elementwise | flops 4096 | bytes 24576 | tf_op jit(solution)/shard_map/reshape | solution.py:475
  6.7 81.4 %layer.1 = bf16[16,512]{1,0:T(8,128)(2,1)} custom-call(bf16[16,4096]{1,0:T(8,128)(2,1)} %tok.1, f32[16,128]{1,0:T(8,128)} %get-tuple-element.6.cosr, f32[16,128]{1,0:T(8,128)} %get-tuple-element.5.sinr, s32[16]{0:T(128)} %lens.1, f32[4,1]{1,0:T(4,128)} %copy.22.lam, f32[1,128]{1,0:T(1,128)} %bitcast.12, f32[1,4096]{1,0:T(1,128)} %bitcast.10, ...), custom_call_target="tpu_custom_call" | custom-call | tf_op jit(solution)/shard_map/layer/pallas_call | solution.py:439
  88.1 1.3 %copy.26 = bf16[16,512]{1,0:T(8,128)(2,1)} copy(bf16[16,512]{1,0:T(8,128)(2,1)} %layer.1) | data formatting | bytes 32768
  (1 shorter events, 0.0 us)

commit v2 on v1

--- a/solution.py
+++ b/solution.py
@@ -1,4 +1,5 @@
 import functools
+import math
 
 import jax
 import jax.numpy as jnp
@@ -35,13 +36,13 @@
 
 def kernel(
     ep, tp, kv, heads,
-    tok, cosr, sinr, lens, lam, hgain, fgain, sgain, ids, rw, dmix,
+    tok, lens, lam, hgain, fgain, sgain, ids, rw, dmix,
     qw, kw, vw, ow, kc, vc, eg, eu, ed, dg, du, dd,
     out,
     wq, wk, wv, wo, kbuf, vbuf, weg, weu, wed, wdg, wdu, wdd,
     cols, sB, rB, qs, ks, vs, hn, heads_all, sD, rD, stat, mixp, sE, rE, arr,
-    sF, rF, sFd, rFd, hG, hGd, acc, sH, rH, mom,
-    wsem, ksem, vsem, esem, ssem, rsem, sdsem, rdsem,
+    sF, rP, sQ, rF, sFd, rPd, sQd, rFd, hG, hGd, acc, sH, rH, mom,
+    wsem, ksem, vsem, esem, ssem, rsem, sdsem, rdsem, psem, qsem,
 ):
     me = lax.axis_index("ep")
     mt = lax.axis_index("tp")
@@ -56,6 +57,36 @@
     fc = eg.shape[2] // tp
     fd = dg.shape[1]
     nrow = 2 * heads
+    nz = tp // 2
+    core = lax.rem(mt, 2)
+    mz = lax.div(mt, 2)
+    sib = mz * 2 + 1 - core
+
+    barrier = pltpu.get_barrier_semaphore()
+
+    def greet(e, t):
+        pl.semaphore_signal(barrier, inc=1, device_id=(e, t), device_id_type=MESH)
+
+    for k in range(1, ep):
+        greet(lax.rem(me + k, ep), mt)
+    for k in range(1, tp):
+        greet(me, lax.rem(mt + k, tp))
+    home_e = lax.div(mt, ratio)
+    for s in range(ep):
+        for h in range(ratio):
+            t = me * ratio + h
+
+            @pl.when((me != s) | (mt != t))
+            def _():
+                greet(s, t)
+
+    for t in range(tp):
+
+        @pl.when((me != home_e) | (mt != t))
+        def _():
+            greet(home_e, t)
+
+    twice = jnp.where(home_e == me, 2 * tp - 2, 2 * tp)
 
     def load(src, dst, sem):
         cp = pltpu.make_async_copy(src, dst, sem)
@@ -65,6 +96,7 @@
     cq = load(qw, wq, wsem.at[0])
     ck = load(kw, wk, wsem.at[1])
     cv = load(vw, wv, wsem.at[2])
+    pl.semaphore_wait(barrier, ep - 1 + tp - 1 + twice)
 
     sends = []
 
@@ -104,14 +136,26 @@
     edc = [load(ed.at[e], wed.at[e], esem.at[2, e]) for e in range(le)]
 
     lane = lax.broadcasted_iota(jnp.int32, (seqs, LANES), 1)
-    idv = [ids[:, k : k + 1] for k in range(TOPK)]
+    diag = lax.broadcasted_iota(jnp.int32, (seqs, seqs), 0) == lax.broadcasted_iota(
+        jnp.int32, (seqs, seqs), 1
+    )
+
+    def upright(row):
+        return jnp.sum(jnp.where(diag, row[:, 0:seqs], 0.0), axis=1, keepdims=True)
+
+    def flat(column):
+        wide = lax.broadcasted_iota(jnp.int32, (seqs, LANES), 0) == lane
+        return jnp.sum(jnp.where(wide, column, 0.0), axis=0, keepdims=True)
+
+    idv = [upright(ids[k : k + 1, :].astype(F32)).astype(jnp.int32) for k in range(TOPK)]
+    rwv = [upright(rw[k : k + 1, :]) for k in range(TOPK)]
     hit = [(lane == i).astype(F32) for i in idv]
     low = (
         lax.broadcasted_iota(jnp.int32, (seqs, seqs), 1)
         < lax.broadcasted_iota(jnp.int32, (seqs, seqs), 0)
     ).astype(BF16)
     earlier = mm(low, (hit[0] + hit[1]).astype(BF16))
-    rsum = rw[:, 0:1] + rw[:, 1:2]
+    rsum = rwv[0] + rwv[1]
     slot_lane = lax.broadcasted_iota(jnp.int32, (seqs, ep * PAD), 1)
     place = jnp.zeros((seqs, ep * PAD), F32)
     mixw = jnp.zeros((seqs, ep * PAD), F32)
@@ -123,7 +167,21 @@
         col = home * PAD + (idv[k] - home * le) * CAP + slot
         eq = (slot_lane == col).astype(F32)
         place = place + eq
-        mixw = mixw + eq * (rw[:, k : k + 1] / rsum)
+        mixw = mixw + eq * (rwv[k] / rsum)
+
+    half = SUB // 2
+    srow = lax.broadcasted_iota(jnp.int32, (seqs, 1), 0)
+    lenc = jnp.zeros((seqs, 1), F32)
+    for s in range(seqs):
+        lenc = jnp.where(srow == s, lens[s].astype(F32), lenc)
+    frequency = jnp.exp((lane & (half - 1)).astype(F32) * (-math.log(theta_base) / half))
+    angles = lenc * frequency
+    cosine = jnp.cos(angles)
+    sine = jnp.where((lane & (SUB - 1)) < half, -1.0, 1.0) * jnp.sin(angles)
+    lamc = jnp.zeros((heads, 1), F32)
+    for h in range(heads):
+        hrow = lax.broadcasted_iota(jnp.int32, (heads, 1), 0)
+        lamc = jnp.where(hrow == h, lam[h], lamc)
 
     cq.wait()
     ck.wait()
@@ -144,7 +202,6 @@
     lane = lax.broadcasted_iota(jnp.int32, (seqs, LANES), 1)
     lower = (lane & (SUB - 1)) < SUB // 2
     first = lane < SUB
-    cosine, sine = cosr[...], sinr[...]
 
     def turned(v):
         up = pltpu.roll(v, LANES - SUB // 2, 1)
@@ -171,7 +228,6 @@
     for r in range(nrow):
         krow = jnp.where(crow == r, (r % heads) // group, krow)
     mine = lax.rem(ccol, kv) == krow if kv > 1 else ccol >= 0
-    lamc = lam[...]
     gain = hgain[...] * head_scale
 
     def one(s):
@@ -246,21 +302,32 @@
     mloc = jnp.mean(resid, axis=1, keepdims=True)
     cent = resid - mloc
     m2 = jnp.sum(cent * cent, axis=1, keepdims=True)
-    stat[mt] = jnp.where(lane == 0, mloc, m2)
+    stat[mt, 0:1] = flat(mloc)
+    stat[mt, 1:2] = flat(m2)
     got = post(3, "tp", lambda p: stat.at[mt], lambda m: stat.at[m])
     arrive(got)
-    mean = stat[0]
+    mean = stat[0, 0:1]
+    sqs = stat[0, 1:2]
     for t in range(1, tp):
-        mean = mean + stat[t]
-    sqs = mean[:, 1:2]
-    mean = mean[:, 0:1] * (1.0 / tp)
+        mean = mean + stat[t, 0:1]
+        sqs = sqs + stat[t, 1:2]
+    mean = mean * (1.0 / tp)
     for t in range(tp):
-        d = stat[t][:, 0:1] - mean
+        d = stat[t, 0:1] - mean
         sqs = sqs + d * d * own
+    mean, sqs = upright(mean), upright(sqs)
     rstd = lax.rsqrt(sqs * (1.0 / width) + layer_epsilon)
     hidden = ((resid - mean) * rstd * fgain[:, aligned(mt, own)]).astype(BF16)
     hidf = hidden.astype(F32)
-    dotp = jnp.sum(hidf * dmix[:, aligned(mt, own)], axis=1, keepdims=True)
+    dmat = dmix[...].astype(F32)
+    drow = lax.broadcasted_iota(jnp.int32, dmat.shape, 0)
+    dotw = jnp.zeros((seqs, LANES), F32)
+    for c in range(own // LANES):
+        pick = jnp.sum(
+            jnp.where(drow == mt * (own // LANES) + c, dmat, 0.0), axis=0, keepdims=True
+        )
+        dotw = dotw + hidf[:, c * LANES : (c + 1) * LANES] * pick
+    dotp = jnp.sum(dotw, axis=1, keepdims=True)
 
     packed = lax.dot_general(
         place, hidf, (((0,), (0,)), ((), ())), preferred_element_type=F32
@@ -269,7 +336,8 @@
         sE[p, 0:seqs] = hidden
         sE[p, seqs : seqs + PAD] = packed[p * PAD : (p + 1) * PAD]
     got = post(4, "ep", lambda p: sE.at[p], lambda m: rE.at[m])
-    mixp[mt] = jnp.broadcast_to(dotp, (seqs, LANES))
+    mixp[mt, 0:1] = flat(dotp)
+    mixp[mt, 1:2] = flat(dotp)
     got_mix = post(5, "tp", lambda p: mixp.at[mt], lambda m: mixp.at[m])
     rE[me] = sE[me]
     nslot = le * slots
@@ -286,58 +354,106 @@
     cdu.wait()
     sFd[:, :, 0:fd] = mm(rows, wdg[...]).reshape(tp, ep * seqs // tp, fd).astype(BF16)
     sFd[:, :, fd:] = mm(rows, wdu[...]).reshape(tp, ep * seqs // tp, fd).astype(BF16)
-    got_d = post(6, "tp", lambda p: sFd.at[p], lambda m: rFd.at[m])
-    rFd[mt] = sFd[mt]
+    def pair(src, dst, kind, k):
+        return pltpu.make_async_remote_copy(
+            src_ref=src, dst_ref=dst,
+            send_sem=psem.at[0, kind, k], recv_sem=psem.at[1, kind, k],
+            device_id=(me, sib), device_id_type=MESH,
+        )
+
+    def along(src, dst, kind, k):
+        return pltpu.make_async_remote_copy(
+            src_ref=src, dst_ref=dst,
+            send_sem=qsem.at[0, kind, k], recv_sem=qsem.at[1, kind, k],
+            device_id=(me, lax.rem(mz + k, nz) * 2 + core), device_id_type=MESH,
+        )
+
+    def zof(k):
+        return lax.rem(mz + k, nz)
+
+    order = list(range(1, nz)) + [0]
+    dpair = [
+        pair(sFd.at[zof(k) * 2 + 1 - core], rPd.at[k], 0, k) for k in range(nz)
+    ]
+    for k in order:
+        dpair[k].start()
     for cp in ecp:
         cp.wait()
 
-    def fcopy(k):
-        peer = lax.rem(mt + k, tp)
-        return pltpu.make_async_remote_copy(
-            src_ref=sF.at[peer], dst_ref=rF.at[mt],
-            send_sem=ssem.at[7, k], recv_sem=rsem.at[7, k],
-            device_id=(me, peer), device_id_type=MESH,
-        )
-
-    def chunk(peer, into):
+    def chunk(peer, into, k):
         for e in range(le):
             xe = arr[e * slots : (e + 1) * slots]
-            into[peer, 0, e * slots : (e + 1) * slots] = mm(
+            into[k, 0, e * slots : (e + 1) * slots] = mm(
                 xe, weg[e, :, aligned(peer, fc)]
             ).astype(BF16)
-            into[peer, 1, e * slots : (e + 1) * slots] = mm(
+            into[k, 1, e * slots : (e + 1) * slots] = mm(
                 xe, weu[e, :, aligned(peer, fc)]
             ).astype(BF16)
 
-    def fstep(k, carry):
-        chunk(lax.rem(mt + k, tp), sF)
-        fcopy(k).start()
-        return carry
-
-    lax.fori_loop(1, tp, fstep, 0)
-    chunk(mt, rF)
-
-    arrive(got_d)
+    epair = [pair(sF.at[k], rP.at[k], 1, k) for k in range(nz)]
+    ealong = [along(sQ.at[k], rF.at[mz], 1, k) for k in range(nz)]
+    dalong = [along(sQd.at[k], rFd.at[mz], 0, k) for k in range(nz)]
+
+    def pass_on(k):
+        epair[k].wait_recv()
+        if k:
+            for j in range(2):
+                sQ[k, j] = (sQ[k, j].astype(F32) + rP[k, j].astype(F32)).astype(BF16)
+            ealong[k].start()
+        else:
+            for j in range(2):
+                rF[mz, j] = (sQ[k, j].astype(F32) + rP[k, j].astype(F32)).astype(BF16)
+
+    for i, k in enumerate(order):
+        z = zof(k)
+        chunk(z * 2 + 1 - core, sF, k)
+        epair[k].start()
+        chunk(z * 2 + core, sQ, k)
+        dpair[k].wait_recv()
+        dboth = (sFd[z * 2 + core].astype(F32) + rPd[k].astype(F32)).astype(BF16)
+        if k:
+            sQd[k] = dboth
+            dalong[k].start()
+        else:
+            rFd[mz] = dboth
+        if i:
+            pass_on(order[i - 1])
+    pass_on(order[-1])
+
+    for k in range(1, nz):
+        dalong[k].wait_recv()
     dsum = rFd[0].astype(F32)
-    for t in range(1, tp):
+    for t in range(1, nz):
         dsum = dsum + rFd[t].astype(F32)
     dg_, du_ = dsum[:, 0:fd], dsum[:, fd:]
     hGd[mt] = (dg_ / (1.0 + jnp.exp(-dg_)) * du_).astype(BF16)
-    got_d = post(8, "tp", lambda p: hGd.at[mt], lambda m: hGd.at[m])
-
-    for k in range(1, tp):
-        fcopy(k).wait_recv()
+
+    def spread(buf, kind):
+        ways = [along(buf.at[mt], buf.at[mt], kind, k) for k in range(nz)]
+        for k in range(1, nz):
+            ways[k].start()
+        hops = []
+        for k in range(nz):
+            z = lax.rem(mz + nz - k, nz) * 2
+            hops.append(pair(buf.at[z + core], buf.at[z + core], kind, k))
+        hops[0].start()
+        return ways, hops
+
+    dways, dhops = spread(hGd, 2)
+
+    for k in range(1, nz):
+        ealong[k].wait_recv()
     gs, us = rF[0, 0].astype(F32), rF[0, 1].astype(F32)
-    for t in range(1, tp):
+    for t in range(1, nz):
         gs = gs + rF[t, 0].astype(F32)
         us = us + rF[t, 1].astype(F32)
     hG[mt] = (gs / (1.0 + jnp.exp(-gs)) * us).astype(BF16)
-    got = post(9, "tp", lambda p: hG.at[mt], lambda m: hG.at[m])
+    ways, hops = spread(hG, 3)
+    for k in range(1, nz):
+        dways[k].wait_recv()
+        dhops[k].start()
 
     cdd.wait()
-    arrive(got_d)
-    dh = hGd[...].astype(F32).reshape(ep * seqs, fd).astype(BF16)
-    sH[:, PAD : PAD + seqs] = mm(dh, wdd[...]).astype(BF16).reshape(ep, seqs, own)
     for cp in edc:
         cp.wait()
 
@@ -347,9 +463,19 @@
 
     acc[...] = jnp.zeros_like(acc)
     down(mt)
-    for k in range(1, tp):
-        got[k - 1].wait_recv()
-        down(lax.rem(mt + tp - k, tp))
+    hops[0].wait_recv()
+    down(sib)
+    for k in range(1, nz):
+        ways[k].wait_recv()
+        hops[k].start()
+        down(lax.rem(mz + nz - k, nz) * 2 + core)
+    for k in range(nz):
+        dhops[k].wait_recv()
+    dh = hGd[...].astype(F32).reshape(ep * seqs, fd).astype(BF16)
+    sH[:, PAD : PAD + seqs] = mm(dh, wdd[...]).astype(BF16).reshape(ep, seqs, own)
+    for k in range(1, nz):
+        hops[k].wait_recv()
+        down(lax.rem(mz + nz - k, nz) * 2 + 1 - core)
     res = acc[...].reshape(nslot, own).astype(BF16)
     back = lax.dot_general(
         perm, res, (((0,), (0,)), ((), ())), preferred_element_type=F32
@@ -361,7 +487,7 @@
     mixs = mixp[0]
     for t in range(1, tp):
         mixs = mixs + mixp[t]
-    gate = 1.0 / (1.0 + jnp.exp(-mixs[:, 0:1]))
+    gate = 1.0 / (1.0 + jnp.exp(-upright(mixs[0:1])))
     arrive(got)
     returned = rH[:, 0:PAD].reshape(ep * PAD, own)
     hi = mixw.astype(BF16)
@@ -376,21 +502,28 @@
     comb = residual_scale * hidf + emix + gate * dout
     s1 = jnp.sum(comb, axis=1, keepdims=True)
     s2 = jnp.sum(comb * comb, axis=1, keepdims=True)
-    mom[mt] = jnp.where(lane == 0, s1, s2)
+    mom[mt, 0:1] = flat(s1)
+    mom[mt, 1:2] = flat(s2)
     got = post(11, "tp", lambda p: mom.at[mt], lambda m: mom.at[m])
     arrive(got)
     ms = mom[0]
     for t in range(1, tp):
         ms = ms + mom[t]
     ms = ms * (1.0 / width)
-    avg = ms[:, 0:1]
-    var = ms[:, 1:2] - avg * avg
+    avg = upright(ms[0:1])
+    var = upright(ms[1:2]) - avg * avg
     out[...] = ((comb - avg) * lax.rsqrt(var + layer_epsilon) * sgain[...]).astype(BF16)
 
     for cp in sends:
         cp.wait_send()
-    for k in range(1, tp):
-        fcopy(k).wait_send()
+    for k in range(nz):
+        dpair[k].wait_send()
+        epair[k].wait_send()
+        hops[k].wait_send()
+        dhops[k].wait_send()
+        if k:
+            for cp in (dalong[k], ealong[k], ways[k], dways[k]):
+                cp.wait_send()
     for ds in range(ep):
         for h in range(ratio):
             t, cp = dcopy(ds, h)
@@ -423,23 +556,17 @@
     slots = ep * CAP
     rows = ep * seqs
     npos = cache * kv
-    lanes = jnp.arange(LANES, dtype=jnp.int32)
-    half = SUB // 2
-    frequency = theta_base ** (-((lanes % half).astype(F32) * (2.0 / SUB)))
-    angles = lengths.astype(F32)[:, None] * frequency[None, :]
-    sign = jnp.where(lanes % SUB < half, -1.0, 1.0)
-    cosine = jnp.cos(angles)
-    sine = jnp.sin(angles) * sign[None, :]
     vm = pl.BlockSpec(memory_space=pltpu.VMEM)
     sm = pl.BlockSpec(memory_space=pltpu.SMEM)
     hb = pl.BlockSpec(memory_space=pl.ANY)
     V = pltpu.VMEM
     D = pltpu.SemaphoreType.DMA
     n = max(ep, tp)
+    nz = tp // 2
     return pl.pallas_call(
         functools.partial(kernel, ep, tp, kv, heads),
         out_shape=jax.ShapeDtypeStruct((seqs, own), BF16),
-        in_specs=[vm] * 3 + [sm] + [vm] * 7 + [hb] * 12,
+        in_specs=[vm, sm, sm] + [vm] * 6 + [hb] * 12,
         out_specs=vm,
         scratch_shapes=[
             V(query_weight.shape, BF16), V(key_weight.shape, BF16), V(value_weight.shape, BF16),
@@ -453,26 +580,29 @@
             V((seqs, heads, LANES), F32), V((seqs, heads, LANES), F32),
             V((ep, seqs, heads * LANES), BF16),
             V((ratio, ep, seqs, own), BF16), V((tp, seqs, own), BF16),
-            V((tp, seqs, LANES), F32), V((tp, seqs, LANES), F32),
+            V((tp, 2, LANES), F32), V((tp, 2, LANES), F32),
             V((ep, seqs + PAD, own), BF16), V((ep, seqs + PAD, own), BF16),
             V((le * slots, own), BF16),
-            V((tp, 2, le * slots, fc), BF16), V((tp, 2, le * slots, fc), BF16),
-            V((tp, rows // tp, 2 * fd), BF16), V((tp, rows // tp, 2 * fd), BF16),
+            V((nz, 2, le * slots, fc), BF16), V((nz, 2, le * slots, fc), BF16),
+            V((nz, 2, le * slots, fc), BF16), V((nz, 2, le * slots, fc), BF16),
+            V((tp, rows // tp, 2 * fd), BF16), V((nz, rows // tp, 2 * fd), BF16),
+            V((nz, rows // tp, 2 * fd), BF16), V((nz, rows // tp, 2 * fd), BF16),
             V((tp, le * slots, fc), BF16), V((tp, rows // tp, fd), BF16),
             V((le, slots, own), F32),
             V((ep, PAD + seqs, own), BF16), V((ep, PAD + seqs, own), BF16),
-            V((tp, seqs, LANES), F32),
+            V((tp, 2, LANES), F32),
             D((7,)), D((seqs,)), D((seqs,)), D((3, le)),
             D((PHASES, n)), D((PHASES, n)), D((ep, ratio)), D((tp,)),
+            D((2, 4, nz)), D((2, 4, nz)),
         ],
         compiler_params=pltpu.CompilerParams(
-            has_side_effects=True, vmem_limit_bytes=62 * 1024 * 1024
+            collective_id=0, has_side_effects=True, vmem_limit_bytes=62 * 1024 * 1024
         ),
         name="layer",
     )(
-        tokens, cosine, sine, lengths, head_lambda.reshape(heads, 1), head_gain.reshape(1, -1),
-        first_gain.reshape(1, -1), second_gain.reshape(1, -1), expert_ids, route_weights,
-        dense_mix.astype(F32).reshape(1, -1),
+        tokens, lengths, head_lambda, head_gain.reshape(1, -1),
+        first_gain.reshape(1, -1), second_gain.reshape(1, -1), expert_ids.T, route_weights.T,
+        dense_mix.reshape(-1, LANES),
         query_weight, key_weight, value_weight, out_weight,
         key_cache.reshape(seqs, npos, vd), value_cache.reshape(seqs, npos, vd),
         expert_gate, expert_up, expert_down, dense_gate, dense_up, dense_down,

time: 89.8 us -> 73.1 us (0.81)
  Pallas kernels: 81.4 us -> 71.5 us
  local copies, waits for them, and re-layouts: 5.36 us -> 1.32 us
  other arithmetic: 2.69 us -> 0 us
    pallas_call x1, Pallas kernels: 81.4 us -> 71.5 us  [on_device(): pl.pallas_call(functools.partial(kernel, ep, tp, kv, heads), out_shape=ja...]
    unnamed x3 -> x1, local copies, waits for them, and re-layouts: 4.02 us -> 1.32 us
    reshape x1 -> x0, local copies, waits for them, and re-layouts: 1.33 us -> none  [on_device(): head_lambda.reshape(heads, 1)]
    reshape x1 -> x0, other arithmetic: 1.3 us -> none  [on_device(): dense_mix.astype(F32).reshape(1, -1)]
where the time goes in v2:
time: 73.1 us; the launch traced here: 72.9 us
  Pallas kernels  71.5 us (98%)
  local copies, waits for them, and re-layouts  1.32 us (2%)
    pallas_call x1, Pallas kernels, on_device(): pl.pallas_call(functools.partial(kernel, ep, tp, kv, heads), out_shape=ja...  71.5 us

profile of v2, /device:TPU:0, one launch (start us, length us, event | category | flops | bytes accessed | tf_op | source)
XLA Modules:
  0.0 72.9 jit_solution(12351754046924489879)
XLA Ops:
  0.0 71.5 %layer.1 = bf16[16,512]{1,0:T(8,128)(2,1)} custom-call(bf16[16,4096]{1,0:T(8,128)(2,1)} %tok.1, s32[16]{0:T(128)} %lens.1, f32[4]{0:T(128)} %lam.1, f32[1,128]{1,0:T(1,128)} %bitcast.15, f32[1,4096]{1,0:T(1,128)} %bitcast.10, f32[1,512]{1,0:T(1,128)} %bitcast.12, s32[2,16]{1,0:T(2,128)} %bitcast.13, f32[2,16]{1,0:T(2,128)} %bitcast.14, ...), custom_call_target="tpu_custom_call" | custom-call | tf_op jit(solution)/shard_map/layer/pallas_call | solution.py:566
  71.5 1.3 %copy.23 = bf16[16,512]{1,0:T(8,128)(2,1)} copy(bf16[16,512]{1,0:T(8,128)(2,1)} %layer.1) | data formatting | bytes 32768
